TPU v7x, 32 devices: a whole 2x2x4 slice. The times are simulated.
32 devices in a mesh: ep: 8 (over z, x), tp: 4 (over y, core).
Axes of the slice: x: 2, y: 2, z: 4, core: 2. Of those that a mesh axis runs over, the one named last changes fastest.
Arguments:
- tokens: bfloat16 [8192, 2048], P(('ep', 'tp')), may hold values from -6 to 6
- norm_gain: bfloat16 [2048], replicated, may hold values from 0.099609375 to 1.8984375
- expert_ids: int32 [8192, 2], P(('ep', 'tp')), may hold values from 0 to 7, all different within a row; in each aligned block of 256 rows (0 to 255, 256 to 511, ...) at most 128 rows name the same one
- group_weight: float32 [8192], P(('ep', 'tp')), may hold values from 0.25 to 1
- expert_logit: float32 [8192, 2], P(('ep', 'tp')), may hold values from -4 to 4
- w_gate: bfloat16 [8, 2048, 1024], P('ep', None, 'tp'), may hold values from -0.125 to 0.125
- w_up: bfloat16 [8, 2048, 1024], P('ep', None, 'tp'), may hold values from -0.125 to 0.125
- w_down: bfloat16 [8, 1024, 2048], P('ep', 'tp')
- final_gain: bfloat16 [2048], P('tp'), may hold values from 0.099609375 to 1.8984375
Outputs:
- normed_out: bfloat16 [8192, 2048], P('ep', 'tp')
Inputs may be any that keep to these rules, and one draw needn't show every extreme that they name: `expert_ids`: the 2 experts of a token differ. Among the rows of one device (aligned blocks of 256 tokens) no expert is named more than 128 times, a bound that some block reaches.
All inputs are finite; a program needn't handle non-finite values.
Results may differ from a plain program's by a relative error of at most 0.0058.
Values may be sent and summed in bfloat16 or wider, within the bound.
A program may use at most 128 MiB of HBM per device.

v0:
```python
import jax
import jax.numpy as jnp
from jax import lax
from jax.sharding import PartitionSpec as P

D = 2048


EPS = 1e-06


def local(
    tokens, norm_gain, expert_ids, group_weight, expert_logit, w_gate, w_up, w_down, final_gain
):
    tok_dev, width = tokens.shape
    per_token = expert_ids.shape[1]
    exp_dev = w_gate.shape[0]
    experts = exp_dev * lax.axis_size("ep")
    capacity = 2 * tok_dev * per_token // experts
    assigned = tok_dev * per_token
    tokens_f = tokens.astype(jnp.float32)
    inverse_in = lax.rsqrt(jnp.mean(tokens_f * tokens_f, axis=-1, keepdims=True) + EPS)
    normed_in = (tokens_f * inverse_in * norm_gain.astype(jnp.float32)).astype(jnp.bfloat16)
    flat_ids = expert_ids.reshape(assigned)
    onehot = (flat_ids[:, None] == jnp.arange(experts, dtype=jnp.int32)[None, :]).astype(jnp.int32)
    before = jnp.cumsum(onehot, axis=0) - onehot
    slot_rank = jnp.sum(before * onehot, axis=1)
    position = slot_rank * experts + flat_ids
    owner_row = (
        jnp.zeros((capacity * experts,), jnp.int32)
        .at[position]
        .set(jnp.arange(assigned, dtype=jnp.int32) // per_token + 1)
    )
    source = normed_in[jnp.maximum(owner_row - 1, 0)]
    outgoing = jnp.where((owner_row > 0)[:, None], source, jnp.zeros_like(source)).reshape(
        capacity, experts, width
    )
    down_whole = lax.all_gather(w_down, "tp", axis=1, tiled=True)
    gate_whole, up_whole = (
        lax.all_gather(w_gate, "tp", axis=2, tiled=True),
        lax.all_gather(w_up, "tp", axis=2, tiled=True),
    )
    incoming = lax.all_to_all(outgoing, "ep", split_axis=1, concat_axis=1, tiled=True)
    item_count = incoming.shape[0]
    senders = incoming.shape[1] // exp_dev
    arranged = incoming.reshape(item_count, senders, exp_dev, width)
    routed = arranged[:, :, 0, :].reshape(item_count * senders, width)
    gate_full = jnp.dot(routed, gate_whole[0], preferred_element_type=jnp.float32)
    up_full = jnp.dot(routed, up_whole[0], preferred_element_type=jnp.float32)
    hidden = (jax.nn.silu(gate_full) * up_full).astype(jnp.bfloat16)
    product = jnp.dot(hidden, down_whole[0], preferred_element_type=jnp.float32).astype(
        jnp.bfloat16
    )
    results = [product.reshape(item_count, senders, width)]
    answer = jnp.stack(results, axis=2).reshape(item_count, senders * exp_dev, width)
    arrived = lax.all_to_all(answer, "ep", split_axis=1, concat_axis=1, tiled=True)
    picked = arrived.reshape(capacity * experts, width)[position].reshape(tok_dev, per_token, width)
    expert_share = jnp.exp(expert_logit)
    expert_share = expert_share / jnp.sum(expert_share, axis=-1, keepdims=True)
    route_weight = group_weight[:, None] * expert_share
    mixture = tokens_f + jnp.sum(route_weight[:, :, None] * picked.astype(jnp.float32), axis=1)
    residual = mixture.astype(jnp.bfloat16)
    sliced = lax.all_to_all(residual, "tp", split_axis=1, concat_axis=0, tiled=True).astype(
        jnp.float32
    )
    squares = lax.psum(jnp.sum(sliced * sliced, axis=-1), "tp")
    inverse_out = lax.rsqrt(squares / D + EPS)
    return (sliced * inverse_out[:, None] * final_gain.astype(jnp.float32)).astype(jnp.bfloat16)


def solution(mesh):
    placed = (
        P(("ep", "tp"), None),
        P(),
        P(("ep", "tp"), None),
        P(("ep", "tp")),
        P(("ep", "tp"), None),
        P("ep", None, "tp"),
        P("ep", None, "tp"),
        P("ep", "tp", None),
        P("tp"),
    )
    return jax.shard_map(
        local, mesh=mesh, in_specs=placed, out_specs=P("ep", "tp"), check_vma=False
    )
```

profile of v0, /device:TPU:11, one launch (start us, length us, event | category | flops | bytes accessed | tf_op | source)
XLA Modules:
  0.0 321.0 jit_solution(3428466047223147058)
XLA Ops:
  6.5 0.0 copy-start
  6.5 0.0 all-gather.6.cloned.1.call-start
  6.5 0.7 all-gather.6.cloned.1.call-update
  7.3 0.0 all-gather.4.cloned.1.call-start
  7.3 0.7 all-gather.4.cloned.1.call-update
  8.0 0.8 copy.29
  8.8 0.1 eq.29
  9.0 1.1 reduce-window.6
  10.1 0.2 slice_reduce_fusion
  10.3 0.1 eq.25
  10.5 0.1 reshape.83
  10.7 0.7 convert_element_type.53
  11.4 0.1 fusion.23
  11.5 2.4 scatter_custom_fusion
  13.9 0.1 broadcast_in_dim.14
  14.0 0.1 copy.32
  14.1 1.5 fusion.16
  15.7 0.0 copy-done
  15.7 0.3 fusion.18
  16.0 6.1 %gather_fusion = bf16[1024,2048]{1,0:T(8,128)(2,1)} fusion(bf16[256,2048]{1,0:T(8,128)(2,1)S(1)} %fusion.18, s32[1024]{0:T(1024)S(1)} %maximum_clamp_fusion), kind=kCustom, calls=%fused_computation | custom fusion | bytes 8392704 | tf_op jit(solution)/shard_map/gather | solution.py:34
  22.1 9.9 %copy_select_fusion = bf16[128,8,2048]{2,0,1:T(8,128)(2,1)} fusion(bf16[128,8,2048]{2,1,0:T(8,128)(2,1)} %bitcast.53, pred[128,8]{0,1:T(8,128)(4,1)S(1)} %copy.32), kind=kLoop, calls=%fused_computation.12 | loop fusion | flops 2097152 | bytes 8389632 | tf_op jit(solution)/shard_map/jit(_where)/select_n | solution.py:35
  32.0 5.7 %all-to-all-start = ((bf16[128,8,2048]{2,0,1:T(8,128)(2,1)}), bf16[128,8,2048]{2,0,1:T(8,128)(2,1)}, u32[]{:S(2)}, u32[]{:S(2)}) async-start(bf16[128,8,2048]{2,0,1:T(8,128)(2,1)} %copy_select_fusion), calls=%async_computation | async-start | bytes 8388608 | tf_op jit(solution)/shard_map/all_to_all | solution.py:43
  37.6 0.0 all-gather.8.cloned.1.call-start
  37.6 0.7 all-gather.8.cloned.1.call-update
  38.4 7.1 %all-gather.6.cloned.1.call-done = bf16[1,2048,1024]{2,1,0:T(8,128)(2,1)} async-done(((bf16[1,2048,256]{2,1,0:T(8,128)(2,1)}), bf16[1,2048,1024]{2,1,0:T(8,128)(2,1)}) %all-gather.6.cloned.1.call-update) | async-done | bytes 4194320 | tf_op jit(solution)/shard_map/all_gather | solution.py:41
  45.5 82.8 %all-to-all-done = bf16[128,8,2048]{2,0,1:T(8,128)(2,1)} async-done(((bf16[128,8,2048]{2,0,1:T(8,128)(2,1)}), bf16[128,8,2048]{2,0,1:T(8,128)(2,1)}, u32[]{:S(2)}, u32[]{:S(2)}) %all-to-all-start) | async-done | bytes 4194336 | tf_op jit(solution)/shard_map/all_to_all | solution.py:43
  128.3 10.3 %fusion.2 = f32[1024,1024]{1,0:T(8,128)} fusion(bf16[1,2048,1024]{2,1,0:T(8,128)(2,1)} %all-gather.6.cloned.1.call-done, bf16[128,8,2048]{2,0,1:T(8,128)(2,1)} %all-to-all-done), kind=kOutput, calls=%fused_computation.5 | convolution fusion | flops 4294967296 | bytes 12582912 | tf_op jit(solution)/shard_map/dot_general | solution.py:49
  138.6 0.0 all-gather.4.cloned.1.call-done
  138.6 11.4 %multiply_convert_fusion = bf16[1024,1024]{1,0:T(8,128)(2,1)} fusion(f32[1024,1024]{1,0:T(8,128)} %fusion.2, bf16[1,2048,1024]{2,1,0:T(8,128)(2,1)} %all-gather.4.cloned.1.call-done, bf16[128,8,2048]{2,0,1:T(8,128)(2,1)} %all-to-all-done), kind=kOutput, calls=%fused_computation.15 | convolution fusion | flops 4301258752 | bytes 14680064 | tf_op jit(solution)/shard_map/dot_general | solution.py:48
  150.0 0.0 all-gather.8.cloned.1.call-done
  150.0 7.3 %convert_bitcast_fusion = bf16[128,8,2048]{2,1,0:T(8,128)(2,1)S(1)} fusion(bf16[1024,1024]{1,0:T(8,128)(2,1)} %multiply_convert_fusion, bf16[1,1024,2048]{2,1,0:T(8,128)(2,1)} %all-gather.8.cloned.1.call-done), kind=kOutput, calls=%fused_computation.14 | convolution fusion | flops 4297064448 | bytes 10485760 | tf_op jit(solution)/shard_map/dot_general | solution.py:51
  157.3 4.5 %copy.35 = bf16[128,8,2048]{2,0,1:T(8,128)(2,1)} copy(bf16[128,8,2048]{2,1,0:T(8,128)(2,1)S(1)} %convert_bitcast_fusion) | data formatting | bytes 8388608 | tf_op jit(solution)/shard_map/reshape;stack;reshape | solution.py:55
  161.8 0.0 copy-start.1
  161.8 0.0 copy-start.3
  161.8 6.6 %all-to-all-start.1 = ((bf16[128,8,2048]{2,0,1:T(8,128)(2,1)}), bf16[128,8,2048]{2,0,1:T(8,128)(2,1)}, u32[]{:S(2)}, u32[]{:S(2)}) async-start(bf16[128,8,2048]{2,0,1:T(8,128)(2,1)} %copy.35), calls=%async_computation.1 | async-start | bytes 8388608 | tf_op jit(solution)/shard_map/all_to_all | solution.py:56
  168.4 0.0 copy-done.1
  168.4 0.0 copy-done.3
  168.5 0.1 copy.28
  168.6 90.4 %all-to-all-done.1 = bf16[128,8,2048]{2,0,1:T(8,128)(2,1)} async-done(((bf16[128,8,2048]{2,0,1:T(8,128)(2,1)}), bf16[128,8,2048]{2,0,1:T(8,128)(2,1)}, u32[]{:S(2)}, u32[]{:S(2)}) %all-to-all-start.1) | async-done | bytes 4194336 | tf_op jit(solution)/shard_map/all_to_all | solution.py:56
  259.1 6.5 %copy.56 = bf16[128,8,2048]{2,1,0:T(8,128)(2,1)} copy(bf16[128,8,2048]{2,0,1:T(8,128)(2,1)} %all-to-all-done.1) | data formatting | bytes 8388608 | tf_op jit(solution)/shard_map/all_to_all | solution.py:56
  265.5 8.0 %gather_fusion.1 = bf16[512,2048]{1,0:T(8,128)(2,1)} fusion(bf16[1024,2048]{1,0:T(8,128)(2,1)} %bitcast.52, s32[1024]{0:T(1024)S(1)} %pad_clamp_fusion), kind=kCustom, calls=%fused_computation.1 | custom fusion | bytes 4196352 | tf_op jit(solution)/shard_map/gather | solution.py:57
  273.5 5.4 %reshape.85 = f32[256,2,2048]{2,1,0:T(2,128)} reshape(bf16[512,2048]{1,0:T(8,128)(2,1)} %gather_fusion.1) | data formatting | bytes 6291456 | tf_op jit(solution)/shard_map/convert_element_type | solution.py:61
  278.9 8.9 %multiply_reduce_fusion = f32[256,2048]{1,0:T(8,128)S(1)} fusion(f32[256,2,2048]{2,1,0:T(2,128)} %reshape.85, f32[256,2]{1,0:T(8,128)S(1)} %copy.28), kind=kLoop, calls=%fused_computation.13 | loop fusion | flops 1572864 | bytes 6293504 | tf_op jit(solution)/shard_map/reduce_sum | solution.py:61
  287.8 0.0 copy-start.2
  287.8 0.3 fusion.19
  288.2 1.1 copy.57
  289.2 4.0 %all-to-all-start.2 = ((bf16[256,4,512]{2,0,1:T(8,128)(2,1)}), bf16[256,4,512]{2,0,1:T(8,128)(2,1)S(1)}, u32[]{:S(2)}, u32[]{:S(2)}) async-start(bf16[256,4,512]{2,0,1:T(8,128)(2,1)} %bitcast.51), calls=%async_computation.2 | async-start | bytes 2097152 | tf_op jit(solution)/shard_map/all_to_all | solution.py:63
  293.2 0.0 copy-done.2
  293.2 13.5 %all-to-all-done.2 = bf16[256,4,512]{2,0,1:T(8,128)(2,1)S(1)} async-done(((bf16[256,4,512]{2,0,1:T(8,128)(2,1)}), bf16[256,4,512]{2,0,1:T(8,128)(2,1)S(1)}, u32[]{:S(2)}, u32[]{:S(2)}) %all-to-all-start.2) | async-done | bytes 1048608 | tf_op jit(solution)/shard_map/all_to_all | solution.py:63
  306.7 0.3 multiply_reduce_fusion.1
  306.9 0.1 copy.40
  307.1 0.1 copy.39
  307.2 6.0 %psum.7 = f32[1024]{0:T(1024)S(1)} all-reduce(f32[1024]{0:T(1024)S(1)} %bitcast.57), channel_id=1, replica_groups=mesh['ep'=8,'tp'=4] {'tp'}, use_global_device_ids=true, to_apply=%region_8.9 | all-reduce | flops 1024 | bytes 8192 | tf_op jit(solution)/shard_map/psum | solution.py:66
  313.1 1.3 fusion.21
  (15 shorter events, 0.1 us)
Async XLA Ops:
  6.5 9.1 %copy-start = (bf16[256,2048]{1,0:T(8,128)(2,1)S(1)}, bf16[256,2048]{1,0:T(8,128)(2,1)}, u32[]{:S(2)}) copy-start(bf16[256,2048]{1,0:T(8,128)(2,1)} %param.9) | copy-start | bytes 3145732
  6.5 39.0 %all-gather.6.cloned.1.call-start = ((), (), s32[]{:S(2)}) async-start(), calls=%async_computation.4 | async-start | bytes 5242880 | tf_op jit(solution)/shard_map/all_gather | solution.py:41
  7.3 131.4 %all-gather.4.cloned.1.call-start = ((), (), s32[]{:S(2)}) async-start(), calls=%async_computation.3 | async-start | bytes 5242880 | tf_op jit(solution)/shard_map/all_gather | solution.py:40
  32.0 96.3 %all-to-all-start = ((bf16[128,8,2048]{2,0,1:T(8,128)(2,1)}), bf16[128,8,2048]{2,0,1:T(8,128)(2,1)}, u32[]{:S(2)}, u32[]{:S(2)}) async-start(bf16[128,8,2048]{2,0,1:T(8,128)(2,1)} %copy_select_fusion), calls=%async_computation | async-start | bytes 8388608 | tf_op jit(solution)/shard_map/all_to_all | solution.py:43
  37.6 112.4 %all-gather.8.cloned.1.call-start = ((), (), s32[]{:S(2)}) async-start(), calls=%async_computation.5 | async-start | bytes 5242880 | tf_op jit(solution)/shard_map/all_gather | solution.py:38
  161.8 6.6 %copy-start.1 = (f32[256,2]{0,1:T(2,128)S(1)}, f32[256,2]{0,1:T(2,128)}, u32[]{:S(2)}) copy-start(f32[256,2]{0,1:T(2,128)} %param.13) | copy-start | bytes 6148
  161.8 6.6 %copy-start.3 = (f32[256]{0:T(256)S(1)}, f32[256]{0:T(256)}, u32[]{:S(2)}) copy-start(f32[256]{0:T(256)} %param.12) | copy-start | bytes 3076
  161.8 97.2 %all-to-all-start.1 = ((bf16[128,8,2048]{2,0,1:T(8,128)(2,1)}), bf16[128,8,2048]{2,0,1:T(8,128)(2,1)}, u32[]{:S(2)}, u32[]{:S(2)}) async-start(bf16[128,8,2048]{2,0,1:T(8,128)(2,1)} %copy.35), calls=%async_computation.1 | async-start | bytes 8388608 | tf_op jit(solution)/shard_map/all_to_all | solution.py:56
  287.8 5.4 %copy-start.2 = (bf16[512]{0:T(512)(128)(2,1)S(1)}, bf16[512]{0:T(512)(128)(2,1)}, u32[]{:S(2)}) copy-start(bf16[512]{0:T(512)(128)(2,1)} %param.17) | copy-start | bytes 3076
  289.2 17.4 %all-to-all-start.2 = ((bf16[256,4,512]{2,0,1:T(8,128)(2,1)}), bf16[256,4,512]{2,0,1:T(8,128)(2,1)S(1)}, u32[]{:S(2)}, u32[]{:S(2)}) async-start(bf16[256,4,512]{2,0,1:T(8,128)(2,1)} %bitcast.51), calls=%async_computation.2 | async-start | bytes 2097152 | tf_op jit(solution)/shard_map/all_to_all | solution.py:63
Sparse Core Ops, SparseCore 0:
  8.9 36.5 all-gather.5
  47.1 34.9 all-gather.3
  83.7 34.4 all-gather.7
where the time goes:
time: 326 us; the launch traced here: 321 us
  waiting for transfers between devices  196 us (60%)
  local copies, waits for them, and re-layouts  35.9 us (11%)
  matrix products  29 us (9%)
  other arithmetic  24.6 us (8%)
  starting transfers between devices  16.3 us (5%)
  between operations  13.3 us (4%)
  blocking collectives  5.97 us (2%)
    all_to_all x1, waiting for transfers between devices, local(): lax.all_to_all(answer, 'ep', split_axis=1, concat_axis=1, tiled=True)  90.4 us
    all_to_all x1, waiting for transfers between devices, local(): lax.all_to_all(outgoing, 'ep', split_axis=1, concat_axis=1, tiled=True)  82.8 us
    all_to_all x1, waiting for transfers between devices, local(): lax.all_to_all(residual, 'tp', split_axis=1, concat_axis=0, tiled=True)  13.5 us
    dot_general x1, matrix products, local(): jnp.dot(routed, gate_whole[0], preferred_element_type=jnp.float32)  11.4 us
    dot_general x1, matrix products, local(): up_full = jnp.dot(routed, up_whole[0], preferred_element_type=jnp.float32)  10.3 us
    select_n x1, other arithmetic, local(): jnp.where((owner_row > 0)[:, None], source, jnp.zeros_like(source))  9.92 us
    reduce_sum x1, other arithmetic, local(): jnp.sum(route_weight[:, :, None] * picked.astype(jnp.float32), axis=1)  8.89 us
    gather x1, local copies, waits for them, and re-layouts, local(): arrived.reshape(capacity * experts, width)[position]  7.96 us
  transfers between devices with their start and end apart: 6, of which 4 were waited for; matrix products, arithmetic and copies ran while one was open for 14% of the time, Pallas kernels for 0%

commit v1 on v0

v1 whole, which is shorter than its diff:
```python
import functools

import jax
import jax.numpy as jnp
from jax import lax
from jax.experimental import pallas as pl
from jax.experimental.pallas import tpu as pltpu
from jax.sharding import PartitionSpec as P

EPS = 1e-06
PAIR = 2
MESH = pl.DeviceIdType.MESH
VMEM = pl.BlockSpec(memory_space=pltpu.VMEM)


def line_gather(line, parts, x_ref, m_ref, o_ref, mo_ref, right_sem, left_sem, recv_sem,
                mright_sem, mleft_sem, mrecv_sem):
    ep = lax.axis_index("ep")
    z = ep // PAIR
    rows = x_ref.shape[0] // parts
    barrier = pltpu.get_barrier_semaphore()

    @pl.when(z > 0)
    def _():
        pl.semaphore_signal(barrier, inc=1, device_id={"ep": ep - PAIR}, device_id_type=MESH)

    @pl.when(z < line - 1)
    def _():
        pl.semaphore_signal(barrier, inc=1, device_id={"ep": ep + PAIR}, device_id_type=MESH)

    pl.semaphore_wait(barrier, jnp.where(z > 0, 1, 0) + jnp.where(z < line - 1, 1, 0))

    def copy(step, part, block, target, sems):
        piece = pl.ds(part * rows, rows)
        source = x_ref.at[piece] if step == 0 else o_ref.at[block, piece]
        return pltpu.make_async_remote_copy(
            src_ref=source, dst_ref=o_ref.at[block, piece], send_sem=sems.at[block, part],
            recv_sem=recv_sem.at[block, part], device_id={"ep": target}, device_id_type=MESH)

    def copy_meta(step, block, target, sems):
        source = m_ref if step == 0 else mo_ref.at[block]
        return pltpu.make_async_remote_copy(
            src_ref=source, dst_ref=mo_ref.at[block], send_sem=sems.at[block],
            recv_sem=mrecv_sem.at[block], device_id={"ep": target}, device_id_type=MESH)

    for step in range(line - 1):
        for part in range(parts):
            for way, sems, msems in ((1, right_sem, mright_sem), (-1, left_sem, mleft_sem)):
                block = z - way * step
                target = ep + way * PAIR
                here = (block >= 0) & (block < line)
                there = (z + way >= 0) & (z + way < line)
                if step > 0:
                    @pl.when(here)
                    def _():
                        copy(step, part, block, target, sems).wait_recv()
                        if part == 0:
                            copy_meta(step, block, target, msems).wait_recv()

                @pl.when(here & there)
                def _():
                    if part == 0:
                        copy_meta(step, block, target, msems).start()
                    copy(step, part, block, target, sems).start()
        if step == 0:
            o_ref[z] = x_ref[...]
            mo_ref[z] = m_ref[...]
    for way, sems, msems in ((1, right_sem, mright_sem), (-1, left_sem, mleft_sem)):
        last = z - way * (line - 1)

        @pl.when((last >= 0) & (last < line))
        def _():
            copy_meta(1, last, ep, msems).wait_recv()
            for part in range(parts):
                copy(1, part, last, ep, sems).wait_recv()

        for step in range(line - 1):
            block = z - way * step

            @pl.when((block >= 0) & (block < line) & (z + way >= 0) & (z + way < line))
            def _():
                copy_meta(step, block, ep, msems).wait_send()
                for part in range(parts):
                    copy(step, part, block, ep, sems).wait_send()


def experts_kernel(line, cap, x_ref, m_ref, gate_ref, up_ref, down_ref, o_ref, rows_ref, acc_ref,
                   pick_ref, weight_ref, part_ref):
    e, j = pl.program_id(0), pl.program_id(1)
    last_e, last_j = pl.num_programs(0) - 1, pl.num_programs(1) - 1
    tok = x_ref.shape[1]

    @pl.when(j == 0)
    def _():
        expert = (lax.axis_index("ep") // PAIR * PAIR + e).astype(jnp.float32)
        earlier = (lax.broadcasted_iota(jnp.int32, (tok, tok), 0)
                   < lax.broadcasted_iota(jnp.int32, (tok, tok), 1)).astype(jnp.bfloat16)
        slot = lax.broadcasted_iota(jnp.int32, (cap, tok), 0).astype(jnp.float32)
        for b in range(line):
            meta = m_ref[b]
            first, second = meta[0:1] == expert, meta[1:2] == expert
            named = jnp.where(first | second, 1.0, 0.0)
            share = jnp.where(first, meta[2:3], 0.0) + jnp.where(second, meta[3:4], 0.0)
            rank = jnp.dot(jnp.broadcast_to(named, (8, tok)).astype(jnp.bfloat16), earlier,
                           preferred_element_type=jnp.float32)[0:1]
            pick = jnp.where(slot == rank, 1.0, 0.0) * named
            weight_ref[b * cap:(b + 1) * cap] = jnp.broadcast_to(
                jnp.sum(pick * share, axis=1, keepdims=True), (cap, 128))
            pick = pick.astype(jnp.bfloat16)
            pick_ref[b * cap:(b + 1) * cap] = pick
            rows_ref[b * cap:(b + 1) * cap] = jnp.dot(
                pick, x_ref[b], preferred_element_type=jnp.float32).astype(jnp.bfloat16)

    rows = rows_ref[...]
    gate = jnp.dot(rows, gate_ref[0, 0], preferred_element_type=jnp.float32)
    up = jnp.dot(rows, up_ref[0, 0], preferred_element_type=jnp.float32)
    hidden = (gate / (1.0 + jnp.exp(-gate)) * up).astype(jnp.bfloat16)
    product = jnp.dot(hidden, down_ref[0, 0], preferred_element_type=jnp.float32)

    @pl.when(j == 0)
    def _():
        acc_ref[...] = product

    @pl.when(j > 0)
    def _():
        acc_ref[...] += product

    @pl.when(j == last_j)
    def _():
        for b in range(line):
            own = slice(b * cap, (b + 1) * cap)
            weighted = (acc_ref[own] * weight_ref[own, 0:1]).astype(jnp.bfloat16)
            spread = lax.dot_general(pick_ref[own], weighted, (((0,), (0,)), ((), ())),
                                     preferred_element_type=jnp.float32)

            @pl.when(e == 0)
            def _():
                part_ref[b] = spread

            @pl.when(e == last_e)
            def _():
                o_ref[b] = (part_ref[b] + spread).astype(jnp.bfloat16)


def line_reduce(line, ways, parts, p_ref, t_ref, o_ref, from_left, from_right, sent, normed,
                right_sem, left_sem, right_recv, left_recv, out_sem, out_recv):
    ep, tp = lax.axis_index("ep"), lax.axis_index("tp")
    z = ep // PAIR
    tok, width = t_ref.shape
    rows, cols = tok // parts, width // ways
    barrier = pltpu.get_barrier_semaphore()

    @pl.when(z > 0)
    def _():
        pl.semaphore_signal(barrier, inc=1, device_id={"ep": ep - PAIR}, device_id_type=MESH)

    @pl.when(z < line - 1)
    def _():
        pl.semaphore_signal(barrier, inc=1, device_id={"ep": ep + PAIR}, device_id_type=MESH)

    for d in range(1, ways):
        pl.semaphore_signal(barrier, inc=1, device_id={"tp": lax.rem(tp + d, ways)}, device_id_type=MESH)
    pl.semaphore_wait(barrier, ways - 1 + jnp.where(z > 0, 1, 0) + jnp.where(z < line - 1, 1, 0))

    lanes = {1: (from_left, right_sem, right_recv), -1: (from_right, left_sem, left_recv)}

    def copy(way, source, block, part, target):
        landing, send, recv = lanes[way]
        piece = pl.ds(part * rows, rows)
        return pltpu.make_async_remote_copy(
            src_ref=source.at[block, piece], dst_ref=landing.at[block, piece],
            send_sem=send.at[block, part], recv_sem=recv.at[block, part],
            device_id={"ep": target}, device_id_type=MESH)

    def copy_out(d, part):
        peer = lax.rem(tp + d, ways)
        return pltpu.make_async_remote_copy(
            src_ref=normed.at[pl.ds(part * rows, rows), pl.ds(pl.multiple_of(peer * cols, cols), cols)],
            dst_ref=o_ref.at[pl.ds(pl.multiple_of(tp * tok + part * rows, rows), rows)],
            send_sem=out_sem.at[d - 1, part], recv_sem=out_recv.at[d - 1, part],
            device_id={"tp": peer}, device_id_type=MESH)

    for step in range(line - 1):
        for part in range(parts):
            piece = slice(part * rows, (part + 1) * rows)
            for way in (1, -1):
                block = line - 1 - step if way == 1 else step
                target = ep + way * PAIR
                ahead = z < block if way == 1 else z > block
                first = z == 0 if way == 1 else z == line - 1
                landing = lanes[way][0]

                @pl.when(first)
                def _():
                    copy(way, p_ref, block, part, target).start()

                @pl.when(ahead & jnp.logical_not(first))
                def _():
                    copy(way, sent, block, part, target).wait_recv()
                    sent[block, piece] = (p_ref[block, piece].astype(jnp.float32)
                                          + landing[block, piece].astype(jnp.float32)).astype(jnp.bfloat16)
                    copy(way, sent, block, part, target).start()

    for part in range(parts):
        piece = slice(part * rows, (part + 1) * rows)
        place = pl.ds(part * rows, rows)
        sent[z, place] = p_ref[z, place]

        @pl.when(z > 0)
        def _():
            copy(1, sent, z, part, ep).wait_recv()

        @pl.when(z < line - 1)
        def _():
            copy(-1, sent, z, part, ep).wait_recv()

        total = t_ref[piece].astype(jnp.float32) + p_ref[z, place].astype(jnp.float32)
        left = jnp.where(z > 0, from_left[z, place].astype(jnp.float32), 0.0)
        right = jnp.where(z < line - 1, from_right[z, place].astype(jnp.float32), 0.0)
        residual = (total + left + right).astype(jnp.bfloat16).astype(jnp.float32)
        inverse = lax.rsqrt(jnp.mean(residual * residual, axis=-1, keepdims=True) + EPS)
        normed[piece] = (residual * inverse).astype(jnp.bfloat16)
        for d in range(1, ways):
            copy_out(d, part).start()
        o_ref[pl.ds(pl.multiple_of(tp * tok + part * rows, rows), rows)] = normed[
            piece, pl.ds(pl.multiple_of(tp * cols, cols), cols)]

    for block in range(line):
        for way in (1, -1):
            ahead = z < block if way == 1 else z > block

            @pl.when(ahead)
            def _():
                for part in range(parts):
                    copy(way, sent, block, part, ep).wait_send()
    for part in range(parts):
        for d in range(1, ways):
            copy_out(d, part).wait_send()
            copy_out(d, part).wait_recv()


def route_shares(group_weight, expert_logit):
    share = jnp.exp(expert_logit)
    share = share / jnp.sum(share, axis=-1, keepdims=True)
    return group_weight[:, None] * share


def norm_in(tokens, norm_gain):
    tokens_f = tokens.astype(jnp.float32)
    inverse = lax.rsqrt(jnp.mean(tokens_f * tokens_f, axis=-1, keepdims=True) + EPS)
    return (tokens_f * inverse * norm_gain.astype(jnp.float32)).astype(jnp.bfloat16)


def on_line(tokens, norm_gain, expert_ids, group_weight, expert_logit, w_gate, w_up, w_down, final_gain):
    tok, width = tokens.shape
    top = expert_ids.shape[1]
    ep_size, ways = lax.axis_size("ep"), lax.axis_size("tp")
    line = ep_size // PAIR
    hidden = w_gate.shape[2]
    cap = 2 * tok * top // ep_size
    parts = 4
    count = ep_size * ways
    groups = [list(range(i, i + PAIR * ways)) for i in range(0, count, PAIR * ways)]
    gather = lambda w: lax.all_gather(w, ("ep", "tp"), axis_index_groups=groups)
    gates, ups, downs = gather(w_gate), gather(w_up), gather(w_down)

    x = norm_in(tokens, norm_gain)
    shares = route_shares(group_weight, expert_logit)
    meta = jnp.concatenate([expert_ids.astype(jnp.float32).T, shares.T, jnp.zeros((8 - 2 * top, tok), jnp.float32)])
    dma = pltpu.SemaphoreType.DMA
    every, every_meta = pl.pallas_call(
        functools.partial(line_gather, line, parts),
        out_shape=(jax.ShapeDtypeStruct((line, tok, width), jnp.bfloat16),
                   jax.ShapeDtypeStruct((line, 8, tok), jnp.float32)),
        in_specs=[VMEM] * 2, out_specs=(VMEM, VMEM),
        scratch_shapes=[dma((line, parts))] * 3 + [dma((line,))] * 3,
        cost_estimate=pl.CostEstimate(flops=60_000_000_000, bytes_accessed=8_000_000, transcendentals=0),
        compiler_params=pltpu.CompilerParams(collective_id=0, has_side_effects=True, vmem_limit_bytes=24 << 20),
        name="line_gather",
    )(x, meta)

    slots = line * cap
    weight_block = lambda shape: pl.BlockSpec((1, 1) + shape, lambda e, j: (e * ways + j, 0, 0, 0))
    whole = lambda shape: pl.BlockSpec(shape, lambda e, j: (0,) * len(shape))
    partial = pl.pallas_call(
        functools.partial(experts_kernel, line, cap),
        out_shape=jax.ShapeDtypeStruct((line, tok, width), jnp.bfloat16),
        grid=(PAIR, ways),
        in_specs=[whole((line, tok, width)), whole((line, 8, tok)), weight_block((width, hidden)),
                  weight_block((width, hidden)), weight_block((hidden, width))],
        out_specs=whole((line, tok, width)),
        scratch_shapes=[pltpu.VMEM((slots, width), jnp.bfloat16), pltpu.VMEM((slots, width), jnp.float32),
                        pltpu.VMEM((slots, tok), jnp.bfloat16), pltpu.VMEM((slots, 128), jnp.float32),
                        pltpu.VMEM((line, tok, width), jnp.float32)],
        cost_estimate=pl.CostEstimate(flops=14_000_000_000, bytes_accessed=30_000_000, transcendentals=1_000_000),
        compiler_params=pltpu.CompilerParams(vmem_limit_bytes=60 << 20),
        name="experts",
    )(every, every_meta, gates, ups, downs)

    block = pltpu.VMEM((line, tok, width), jnp.bfloat16)
    out = pl.pallas_call(
        functools.partial(line_reduce, line, ways, parts),
        out_shape=jax.ShapeDtypeStruct((ways * tok, width // ways), jnp.bfloat16),
        in_specs=[VMEM] * 2, out_specs=VMEM,
        scratch_shapes=[block, block, block, pltpu.VMEM((tok, width), jnp.bfloat16)]
        + [dma((line, parts))] * 4 + [dma((ways - 1, parts))] * 2,
        compiler_params=pltpu.CompilerParams(collective_id=1, has_side_effects=True, vmem_limit_bytes=40 << 20),
        name="line_reduce",
    )(partial, tokens)
    return (out.astype(jnp.float32) * final_gain.astype(jnp.float32)).astype(jnp.bfloat16)


def by_exchange(tokens, norm_gain, expert_ids, group_weight, expert_logit, w_gate, w_up, w_down, final_gain):
    tok_dev, width = tokens.shape
    per_token = expert_ids.shape[1]
    exp_dev = w_gate.shape[0]
    experts = exp_dev * lax.axis_size("ep")
    capacity = 2 * tok_dev * per_token // experts
    assigned = tok_dev * per_token
    tokens_f = tokens.astype(jnp.float32)
    normed_in = norm_in(tokens, norm_gain)
    flat_ids = expert_ids.reshape(assigned)
    onehot = (flat_ids[:, None] == jnp.arange(experts, dtype=jnp.int32)[None, :]).astype(jnp.int32)
    before = jnp.cumsum(onehot, axis=0) - onehot
    position = jnp.sum(before * onehot, axis=1) * experts + flat_ids
    owner_row = (
        jnp.zeros((capacity * experts,), jnp.int32)
        .at[position]
        .set(jnp.arange(assigned, dtype=jnp.int32) // per_token + 1)
    )
    source = normed_in[jnp.maximum(owner_row - 1, 0)]
    outgoing = jnp.where((owner_row > 0)[:, None], source, jnp.zeros_like(source)).reshape(capacity, experts, width)
    down_whole = lax.all_gather(w_down, "tp", axis=1, tiled=True)
    gate_whole = lax.all_gather(w_gate, "tp", axis=2, tiled=True)
    up_whole = lax.all_gather(w_up, "tp", axis=2, tiled=True)
    incoming = lax.all_to_all(outgoing, "ep", split_axis=1, concat_axis=1, tiled=True)
    senders = incoming.shape[1] // exp_dev
    arranged = incoming.reshape(capacity, senders, exp_dev, width)
    results = []
    for e in range(exp_dev):
        routed = arranged[:, :, e, :].reshape(capacity * senders, width)
        gate = jnp.dot(routed, gate_whole[e], preferred_element_type=jnp.float32)
        up = jnp.dot(routed, up_whole[e], preferred_element_type=jnp.float32)
        hidden = (jax.nn.silu(gate) * up).astype(jnp.bfloat16)
        product = jnp.dot(hidden, down_whole[e], preferred_element_type=jnp.float32).astype(jnp.bfloat16)
        results.append(product.reshape(capacity, senders, width))
    answer = jnp.stack(results, axis=2).reshape(capacity, senders * exp_dev, width)
    arrived = lax.all_to_all(answer, "ep", split_axis=1, concat_axis=1, tiled=True)
    picked = arrived.reshape(capacity * experts, width)[position].reshape(tok_dev, per_token, width)
    shares = route_shares(group_weight, expert_logit)
    mixture = tokens_f + jnp.sum(shares[:, :, None] * picked.astype(jnp.float32), axis=1)
    residual = mixture.astype(jnp.bfloat16)
    sliced = lax.all_to_all(residual, "tp", split_axis=1, concat_axis=0, tiled=True).astype(jnp.float32)
    squares = lax.psum(jnp.sum(sliced * sliced, axis=-1), "tp")
    inverse_out = lax.rsqrt(squares / width + EPS)
    return (sliced * inverse_out[:, None] * final_gain.astype(jnp.float32)).astype(jnp.bfloat16)


def solution(mesh):
    placed = (
        P(("ep", "tp"), None),
        P(),
        P(("ep", "tp"), None),
        P(("ep", "tp")),
        P(("ep", "tp"), None),
        P("ep", None, "tp"),
        P("ep", None, "tp"),
        P("ep", "tp", None),
        P("tp"),
    )

    def local(*args):
        ep_size = mesh.shape["ep"]
        short = ep_size % PAIR == 0 and 2 <= ep_size // PAIR <= 4 and args[5].shape[0] == 1
        return (on_line if short else by_exchange)(*args)

    return jax.shard_map(local, mesh=mesh, in_specs=placed, out_specs=P("ep", "tp"), check_vma=False)
```

time: 326 us -> 296 us (0.908); the launches traced: 321 us -> 296 us
  Pallas kernels: 0 us -> 178 us
  waiting for transfers between devices: 196 us -> 98.1 us
  local copies, waits for them, and re-layouts: 35.9 us -> 4.87 us
  matrix products: 29 us -> 0 us
  other arithmetic: 24.6 us -> 1.89 us
  starting transfers between devices: 16.3 us -> 0.11 us
  blocking collectives: 5.97 us -> 0 us
    all_to_all x3 -> x0, waiting for transfers between devices: 187 us -> none  [the longest x1 90.4 us: local(): lax.all_to_all(answer, 'ep', split_axis=1, concat_axis=1, tiled=True)]
    pallas_call x0 -> x3, Pallas kernels: none -> 178 us  [the longest x1 78.2 us: on_line(): pl.pallas_call(functools.partial(line_reduce, line, ways, parts), out_sha...]
    all_gather x3, waiting for transfers between devices: 7.15 us -> 96 us  [on_line(): gather = lambda w: lax.all_gather(w, ('ep', 'tp'), axis_index_groups=groups)]
    dot_general x3 -> x0, matrix products: 29 us -> none  [the longest x1 11.4 us: local(): jnp.dot(routed, gate_whole[0], preferred_element_type=jnp.float32)]
    all_to_all x3 -> x0, starting transfers between devices: 16.2 us -> none  [the longest x1 6.59 us: local(): lax.all_to_all(answer, 'ep', split_axis=1, concat_axis=1, tiled=True)]
    gather x2 -> x0, local copies, waits for them, and re-layouts: 14 us -> none  [the longest x1 7.96 us: local(): arrived.reshape(capacity * experts, width)[position]]
    reduce_sum x5 -> x2, other arithmetic: 10.8 us -> 0.31 us  [the longest x1 0.29 us: norm_in(): jnp.mean(tokens_f * tokens_f, axis=-1, keepdims=True) + EPS]
    select_n x2 -> x0, other arithmetic: 9.93 us -> none  [the longest x1 9.92 us: local(): jnp.where((owner_row > 0)[:, None], source, jnp.zeros_like(source))]
  transfers between devices with their start and end apart: 6 -> 3, of which waited for: 4 -> 2; matrix products, arithmetic and copies ran while one was open for 14% -> 0% of each run, Pallas kernels for 0% -> 23%
where the time goes in v1:
time: 296 us
  Pallas kernels  178 us (60%)
  waiting for transfers between devices  98.1 us (33%)
  between operations  13.2 us (4%)
  local copies, waits for them, and re-layouts  4.87 us (2%)
    all_gather x3, waiting for transfers between devices, on_line(): gather = lambda w: lax.all_gather(w, ('ep', 'tp'), axis_index_groups=groups)  96 us
    pallas_call x1, Pallas kernels, on_line(): pl.pallas_call(functools.partial(line_reduce, line, ways, parts), out_sha...  78.2 us
    pallas_call x1, Pallas kernels, on_line(): pl.pallas_call(functools.partial(line_gather, line, parts), out_shape=(ja...  69.2 us
    pallas_call x1, Pallas kernels, on_line(): pl.pallas_call(functools.partial(experts_kernel, line, cap), out_shape=ja...  30.7 us
  transfers between devices with their start and end apart: 3, of which 2 were waited for; matrix products, arithmetic and copies ran while one was open for 0% of the time, Pallas kernels for 23%

profile of v1, /device:TPU:11, one launch (start us, length us, event | category | flops | bytes accessed | tf_op | source)
XLA Modules:
  0.0 296.3 jit_solution(6566685804622632246)
XLA Ops:
  6.5 0.0 copy-start.5
  6.5 0.0 copy-start.7
  6.5 0.0 copy-start.4
  6.5 0.0 copy-start
  6.5 0.0 copy-start.6
  6.5 0.0 copy-start.8
  6.6 0.0 all-gather.7.cloned.1.call-start
  6.6 0.7 all-gather.7.cloned.1.call-update
  7.3 0.0 all-gather.9.cloned.1.call-start
  7.3 0.7 all-gather.9.cloned.1.call-update
  8.0 0.0 all-gather.11.cloned.1.call-start
  8.1 0.7 all-gather.11.cloned.1.call-update
  8.8 0.0 copy-done.5
  8.8 0.0 copy-done.7
  8.8 0.1 pad.2.clone
  8.9 0.0 copy-done.4
  8.9 0.0 copy-done
  8.9 0.3 fusion
  9.2 0.0 copy-done.6
  9.3 0.0 copy-done.8
  9.3 0.1 maximum_maximum_fusion.m_ref
  9.4 0.3 fusion.2.x_ref
  9.7 69.2 %line_gather.1 = (bf16[4,256,2048]{2,1,0:T(8,128)(2,1)S(1)}, f32[4,8,256]{2,1,0:T(8,128)S(1)}) custom-call(bf16[256,2048]{1,0:T(8,128)(2,1)S(1)} %fusion.2.x_ref, f32[8,256]{1,0:T(8,128)S(1)} %maximum_maximum_fusion.m_ref), custom_call_target="tpu_custom_call" | custom-call | flops 60000002048 | bytes 8000000 | tf_op jit(solution)/shard_map/line_gather/pallas_call | solution.py:271
  78.9 0.0 copy-start.2
  78.9 2.0 copy-done.2
  80.8 0.0 copy-start.3
  80.8 0.6 copy-done.3
  81.5 0.0 all-gather.7.cloned.1.call-done
  81.5 39.8 %all-gather.9.cloned.1.call-done = bf16[8,2048,256]{2,1,0:T(8,128)(2,1)} async-done(((bf16[1,2048,256]{2,1,0:T(8,128)(2,1)}), bf16[8,2048,256]{2,1,0:T(8,128)(2,1)}) %all-gather.9.cloned.1.call-update) | async-done | bytes 8388624 | tf_op jit(solution)/shard_map/all_gather | solution.py:264
  121.3 56.2 %all-gather.11.cloned.1.call-done = bf16[8,256,2048]{2,1,0:T(8,128)(2,1)} async-done(((bf16[1,256,2048]{2,1,0:T(8,128)(2,1)}), bf16[8,256,2048]{2,1,0:T(8,128)(2,1)}) %all-gather.11.cloned.1.call-update) | async-done | bytes 8388624 | tf_op jit(solution)/shard_map/all_gather | solution.py:264
  177.5 30.7 %experts.1.p_ref = bf16[4,256,2048]{2,1,0:T(8,128)(2,1)} custom-call(bf16[4,256,2048]{2,1,0:T(8,128)(2,1)} %copy-done.2, f32[4,8,256]{2,1,0:T(8,128)} %copy-done.3, bf16[8,1,2048,256]{3,2,1,0:T(8,128)(2,1)} %bitcast.7, bf16[8,1,2048,256]{3,2,1,0:T(8,128)(2,1)} %bitcast.8, bf16[8,1,256,2048]{3,2,1,0:T(8,128)(2,1)} %bitcast.9), custom_call_target="tpu_custom_call" | custom-call | flops 14000000000 | bytes 30000000 | tf_op jit(solution)/shard_map/experts/pallas_call | solution.py:285
  208.2 0.0 copy-start.1
  208.2 2.2 copy-done.1
  210.3 78.2 %line_reduce.1 = bf16[1024,512]{1,0:T(8,128)(2,1)S(1)} custom-call(bf16[4,256,2048]{2,1,0:T(8,128)(2,1)S(1)} %copy-done.1, bf16[256,2048]{1,0:T(8,128)(2,1)S(1)} %copy-done), custom_call_target="tpu_custom_call" | custom-call | tf_op jit(solution)/shard_map/line_reduce/pallas_call | solution.py:301
  288.6 1.2 multiply_convert_fusion
  (7 shorter events, 0.1 us)
Async XLA Ops:
  6.5 2.2 copy-start.5
  6.5 2.3 copy-start.7
  6.5 2.4 copy-start.4
  6.5 2.4 copy-start
  6.5 2.7 copy-start.6
  6.5 2.7 copy-start.8
  6.6 74.9 %all-gather.7.cloned.1.call-start = ((), (), s32[]{:S(2)}) async-start(), calls=%async_computation | async-start | bytes 9437184 | tf_op jit(solution)/shard_map/all_gather | solution.py:264
  7.3 114.0 %all-gather.9.cloned.1.call-start = ((), (), s32[]{:S(2)}) async-start(), calls=%async_computation.1 | async-start | bytes 9437184 | tf_op jit(solution)/shard_map/all_gather | solution.py:264
  8.0 169.4 %all-gather.11.cloned.1.call-start = ((), (), s32[]{:S(2)}) async-start(), calls=%async_computation.2 | async-start | bytes 9437184 | tf_op jit(solution)/shard_map/all_gather | solution.py:264
  78.9 2.0 copy-start.2
  80.8 0.6 copy-start.3
  208.2 2.2 copy-start.1
Sparse Core Ops, SparseCore 0:
  9.3 55.7 all-gather.6
  67.0 54.2 all-gather.8
  123.2 54.2 all-gather.10
